TPU v7x, 32 devices: a whole 2x2x4 slice. The times are simulated.
32 devices in a mesh: grp: 2 (over y), sp: 16 (over z, x, core), tp: 1.
Axes of the slice: x: 2, y: 2, z: 4, core: 2. Of those that a mesh axis runs over, the one named last changes fastest.
Arguments:
- glu_value: bfloat16 [4096, 2048], P(('grp', 'sp'), 'tp'), parts along dimension 0, may hold values from -6 to 6
- glu_gate: bfloat16 [4096, 2048], P(('grp', 'sp'), 'tp'), parts along dimension 0, may hold values from -9 to 9
- segments: int32 [4096], P(('grp', 'sp')), parts along dimension 0, may hold values from 0 to 3, never falling along the last dimension, each value on 1 to 1024 neighbouring positions
- conv_kernel: float32 [31, 2048], P(None, 'tp'), may hold values from -3.5 to 3.5
- norm_gain: float32 [2048], P('tp'), may hold values from 0.1 to 1.9
- norm_bias: float32 [2048], P('tp'), may hold values from -3 to 3
- residual: bfloat16 [4096, 2048], P(('grp', 'sp'), 'tp'), parts along dimension 0, may hold values from -6 to 6
- out_weight: bfloat16 [2048, 2048], P('tp'), may hold values from -0.125 to 0.125
- rms_gain: float32 [2048], replicated, may hold values from 0.1 to 1.9
- experts: int32 [4096, 4], P(('grp', 'sp')), parts along dimension 0, may hold values from 0 to 15, all different within a row; in each aligned block of 128 rows (0 to 127, 128 to 255, ...) at most 64 rows name the same one
- route_weights: float32 [4096, 4], P(('grp', 'sp')), parts along dimension 0, may hold values from 0.1 to 1
- glu_weight: bfloat16 [16, 2048, 2048], P('sp', None, 'tp'), may hold values from -0.5 to 0.5
- lin_weight: bfloat16 [16, 2048, 2048], P('sp', None, 'tp'), may hold values from -0.5 to 0.5
- down_weight: bfloat16 [16, 2048, 2048], P('sp', None, 'tp'), may hold values from -0.015625 to 0.015625
Outputs:
- layer_output: bfloat16 [4096, 2048], P(('grp', 'sp'), 'tp'), parts along dimension 0
There are 2 independent parts, one for each index of `grp`. A program takes and returns all parts, laid end to end along the dimension named above; an argument that names none is the same for every part. Nothing has to cross between parts.
Inputs may be any that keep to these rules, and one draw needn't show every extreme that they name: Each row names 4 different experts. In each aligned block of 128 rows no expert is named by more than 64 rows, and in some block an expert is named by exactly 64 rows. `segments`: never falling along positions; a document holds from 1 up to 1024 positions, and one holds exactly that many.
All inputs are finite; a program needn't handle non-finite values.
Results may differ from a plain program's by a relative error of at most 0.017.
Values may be sent and summed in bfloat16 or wider, within the bound.
A program may use at most 128 MiB of HBM per device.

v0:
```python
import jax
import jax.numpy as jnp
from jax import lax
from jax.sharding import PartitionSpec as P

EPSILON = 1e-05
CLAMP_LIMIT = 7.0
SIGMOID_SCALE = 1.702


def passed_along(array, axis, by):
    length = lax.axis_size(axis)
    pairs = [(i, i + by) for i in range(length) if 0 <= i + by < length]
    return lax.ppermute(array, axis, pairs)


def clamped_unit(gate_pre, lin_pre):
    gate_clip = jnp.minimum(gate_pre, CLAMP_LIMIT)
    linear = jnp.clip(lin_pre, -CLAMP_LIMIT, CLAMP_LIMIT)
    return gate_clip * jax.nn.sigmoid(SIGMOID_SCALE * gate_clip) * (linear + 1.0)


def shards(
    glu_value,
    glu_gate,
    segments,
    conv_kernel,
    norm_gain,
    norm_bias,
    residual,
    out_weight,
    rms_gain,
    experts,
    route_weights,
    glu_weight,
    lin_weight,
    down_weight,
):
    tok_count = glu_value.shape[0]
    local_width = glu_value.shape[1]
    model_width = out_weight.shape[1]
    kernel_reach = conv_kernel.shape[0] - 1
    top_count = experts.shape[1]
    local_experts = glu_weight.shape[0]
    sp_count = lax.axis_size("sp")
    expert_total = local_experts * sp_count
    capacity = min(tok_count, 2 * tok_count * top_count // expert_total)
    glu_out = (glu_value.astype(jnp.float32) * jax.nn.sigmoid(glu_gate.astype(jnp.float32))).astype(
        jnp.bfloat16
    )
    prev_rows, prev_segments = passed_along(
        (glu_out[tok_count - kernel_reach :], segments[tok_count - kernel_reach :]), "sp", 1
    )
    padded = jnp.concatenate([prev_rows, glu_out], axis=0).astype(jnp.float32)
    padded_segments = jnp.concatenate([prev_segments, segments], axis=0)
    conv_sum = jnp.zeros((tok_count, local_width), jnp.float32)
    for offset in range(kernel_reach + 1):
        lower = kernel_reach - offset
        window_rows = padded[lower : lower + tok_count]
        same_document = (padded_segments[lower : lower + tok_count] == segments).astype(jnp.float32)
        conv_sum = conv_sum + conv_kernel[offset][None, :] * window_rows * same_document[:, None]
    row_total, row_square = lax.psum(
        (jnp.sum(conv_sum, axis=1), jnp.sum(conv_sum * conv_sum, axis=1)), "tp"
    )
    row_mean = row_total / model_width
    row_var = row_square / model_width - row_mean * row_mean
    normed_conv = (conv_sum - row_mean[:, None]) * lax.rsqrt(row_var + EPSILON)[
        :, None
    ] * norm_gain + norm_bias
    swished = jax.nn.silu(normed_conv).astype(jnp.bfloat16)
    projected = jnp.dot(swished, out_weight, preferred_element_type=jnp.float32)
    conv_out = lax.psum_scatter(
        projected.astype(jnp.bfloat16), "tp", scatter_dimension=1, tiled=True
    ).astype(jnp.float32)
    updated = (residual.astype(jnp.float32) + conv_out).astype(jnp.bfloat16)
    updated_float = updated.astype(jnp.float32)
    flat_experts = experts.reshape(-1)
    one_hot = (flat_experts[:, None] == jnp.arange(expert_total, dtype=jnp.int32)[None, :]).astype(
        jnp.int32
    )
    slot_rank = jnp.sum((jnp.cumsum(one_hot, axis=0) - 1) * one_hot, axis=1)
    slot_index = flat_experts * capacity + slot_rank
    token_order = jnp.arange(tok_count * top_count, dtype=jnp.int32) // top_count
    slot_token = (
        jnp.full((expert_total * capacity,), tok_count, jnp.int32).at[slot_index].set(token_order)
    )
    whole_rows = lax.all_gather(updated, "tp", axis=1, tiled=True)
    whole_float = whole_rows.astype(jnp.float32)
    normed = (
        whole_float
        * lax.rsqrt(jnp.mean(whole_float * whole_float, axis=1, keepdims=True) + EPSILON)
        * rms_gain
    ).astype(jnp.bfloat16)
    normed_pad = jnp.concatenate([normed, jnp.zeros((1, model_width), jnp.bfloat16)], axis=0)
    packed = normed_pad[slot_token].reshape(sp_count, local_experts, capacity, model_width)
    arrived = lax.all_to_all(packed, "sp", split_axis=0, concat_axis=0, tiled=True)
    gate_pre = jnp.einsum("slmd,ldf->slmf", arrived, glu_weight, preferred_element_type=jnp.float32)
    lin_pre = jnp.einsum("slmd,ldf->slmf", arrived, lin_weight, preferred_element_type=jnp.float32)
    hidden = clamped_unit(gate_pre, lin_pre).astype(jnp.bfloat16)
    summed = jnp.einsum(
        "slmf,lfd->slmd",
        lax.all_gather(hidden, "tp", axis=3, tiled=True),
        down_weight,
        preferred_element_type=jnp.float32,
    )
    results = summed.astype(jnp.bfloat16)
    returned = lax.all_to_all(results, "sp", split_axis=0, concat_axis=0, tiled=True)
    flat_back = returned.reshape(expert_total * capacity, local_width)
    picked = flat_back[slot_index].reshape(tok_count, top_count, local_width).astype(jnp.float32)
    routed_sum = jnp.sum(picked * route_weights[:, :, None], axis=1)
    return (updated_float + routed_sum).astype(jnp.bfloat16)


def solution(mesh):
    in_specs = (
        P(("grp", "sp"), "tp"),
        P(("grp", "sp"), "tp"),
        P(("grp", "sp")),
        P(None, "tp"),
        P("tp"),
        P("tp"),
        P(("grp", "sp"), "tp"),
        P("tp", None),
        P(),
        P(("grp", "sp"), None),
        P(("grp", "sp"), None),
        P("sp", None, "tp"),
        P("sp", None, "tp"),
        P("sp", None, "tp"),
    )
    out_specs = P(("grp", "sp"), "tp")
    return jax.shard_map(shards, mesh=mesh, in_specs=in_specs, out_specs=out_specs, check_vma=False)
```

profile of v0, /device:TPU:11, one launch (start us, length us, event | category | flops | bytes accessed | tf_op | source)
XLA Modules:
  0.0 289.5 jit_solution(576064054343517301)
XLA Ops:
  0.7 3.7 %collective-permute-start.1 = (s32[30]{0:T(128)S(1)}, s32[30]{0:T(128)S(1)}, u32[]{:S(2)}, u32[]{:S(2)}) collective-permute-start(s32[30]{0:T(128)S(1)} %slice.293), channel_id=1, source_target_pairs={{0,1},{1,2},{2,3},{3,4},{4,5},{5,6},{6,7},{7,8},{8,9},{9,10},{10,1... | collective-permute-start | bytes 368 | tf_op jit(solution)/shard_map/ppermute | solution.py:14
  4.5 1.5 multiply_convert_fusion.2
  6.0 1.9 collective-permute-start
  7.9 2.0 fusion.119
  9.9 1.5 fusion.120
  11.4 0.8 copy.22
  13.1 1.2 reduce-window.6
  14.8 2.4 scatter_custom_fusion
  17.3 0.7 pad_add_fusion
  18.0 0.7 compare_convert_fusion.29
  18.8 0.7 compare_convert_fusion.28
  19.8 6.1 %fusion.117 = (f32[128]{0:T(128)S(1)}, f32[128]{0:T(128)S(1)}, f32[128,2048]{1,0:T(8,128)S(1)}) fusion(f32[128]{0:T(128)S(1)} %get-tuple-element.67, f32[158,2048]{1,0:T(8,128)S(1)} %maximum_convert_fusion, f32[2048]{0:T(1024)S(1)} %bitcast.165, f32[128]{0:T(128)S(1)} %get-tuple-element.68, f32[2048]{0:T(1024)S(1)} %bitcast.166, ...), kind=kLoop, calls=%fused_computation.196 | loop fusion | flops 24641280 | bytes 33824768 | tf_op jit(solution)/shard_map/reduce_sum | solution.py:63
  26.0 1.8 multiply_reduce_fusion.1
  28.0 6.0 %gather_fusion = bf16[1024,2048]{1,0:T(8,128)(2,1)} fusion(bf16[129,2048]{1,0:T(8,128)(2,1)S(1)} %concatenate.11, s32[1024]{0:T(1024)S(1)} %fusion.106), kind=kCustom, calls=%fused_computation | custom fusion | bytes 8392704 | tf_op jit(solution)/shard_map/gather | solution.py:95
  34.0 97.6 %all_to_all.10 = bf16[16,1,64,2048]{3,2,1,0:T(8,128)(2,1)S(1)} all-to-all(bf16[16,1,64,2048]{3,2,1,0:T(8,128)(2,1)} %bitcast.135), channel_id=1, replica_groups=mesh['grp'=2,'sp'=16,'tp'=1] {'sp'}, dimensions={0} | all-to-all | bytes 8388608 | tf_op jit(solution)/shard_map/all_to_all | solution.py:96
  131.6 2.0 copy-done
  133.6 13.2 %fusion.9 = f32[16,64,2048]{2,1,0:T(8,128)} fusion(bf16[1,2048,2048]{2,1,0:T(8,128)(2,1)} %param.25, bf16[16,1,64,2048]{3,2,1,0:T(8,128)(2,1)S(1)} %all_to_all.10), kind=kOutput, calls=%fused_computation.15 | convolution fusion | flops 8589934592 | bytes 20971520 | tf_op jit(solution)/shard_map/slmd,ldf->slmf/dot_general | solution.py:97
  146.7 28.4 %convert_bitcast_fusion = bf16[16,1,64,2048]{3,2,1,0:T(8,128)(2,1)} fusion(bf16[1,2048,2048]{2,1,0:T(8,128)(2,1)} %param.27, bf16[1,2048,2048]{2,1,0:T(8,128)(2,1)} %param.26, f32[16,64,2048]{2,1,0:T(8,128)} %fusion.9, bf16[16,1,64,2048]{3,2,1,0:T(8,128)(2,1)} %copy-done), kind=kOutput, calls=%fused_computation.21 | convolution fusion | flops 17202937856 | bytes 33554432 | tf_op jit(solution)/shard_map/slmf,lfd->slmd/dot_general | solution.py:100
  175.1 5.3 %all-to-all-start.1 = ((bf16[16,1,64,2048]{3,2,1,0:T(8,128)(2,1)}), bf16[16,1,64,2048]{3,2,1,0:T(8,128)(2,1)}, u32[]{:S(2)}, u32[]{:S(2)}) async-start(bf16[16,1,64,2048]{3,2,1,0:T(8,128)(2,1)} %convert_bitcast_fusion), calls=%async_computation.1 | async-start | bytes 8388608 | tf_op jit(solution)/shard_map/all_to_all | solution.py:107
  180.6 92.3 %all-to-all-done.1 = bf16[16,1,64,2048]{3,2,1,0:T(8,128)(2,1)} async-done(((bf16[16,1,64,2048]{3,2,1,0:T(8,128)(2,1)}), bf16[16,1,64,2048]{3,2,1,0:T(8,128)(2,1)}, u32[]{:S(2)}, u32[]{:S(2)}) %all-to-all-start.1) | async-done | bytes 4194336 | tf_op jit(solution)/shard_map/all_to_all | solution.py:107
  272.9 7.1 %gather_fusion.1 = bf16[512,2048]{1,0:T(8,128)(2,1)S(1)} fusion(bf16[1024,2048]{1,0:T(8,128)(2,1)} %bitcast.56, s32[1024]{0:T(1024)S(1)} %pad_clamp_fusion), kind=kCustom, calls=%fused_computation.1 | custom fusion | bytes 4196352 | tf_op jit(solution)/shard_map/gather | solution.py:109
  280.1 3.0 %reshape.146 = f32[128,4,2048]{2,1,0:T(4,128)} reshape(bf16[512,2048]{1,0:T(8,128)(2,1)S(1)} %gather_fusion.1) | data formatting | bytes 6291456 | tf_op jit(solution)/shard_map/convert_element_type | solution.py:109
  283.1 5.4 %multiply_reduce_fusion = f32[128,2048]{1,0:T(8,128)S(1)} fusion(f32[128,4,2048]{2,1,0:T(4,128)} %reshape.146, f32[128,4]{1,0:T(8,128)S(1)} %copy.27), kind=kLoop, calls=%fused_computation.20 | loop fusion | flops 1835008 | bytes 5244928 | tf_op jit(solution)/shard_map/reduce_sum | solution.py:110
  288.5 0.9 add_convert_fusion
  (40 shorter events, 2.8 us)
Async XLA Ops:
  0.7 16.6 %collective-permute-start.1 = (s32[30]{0:T(128)S(1)}, s32[30]{0:T(128)S(1)}, u32[]{:S(2)}, u32[]{:S(2)}) collective-permute-start(s32[30]{0:T(128)S(1)} %slice.293), channel_id=1, source_target_pairs={{0,1},{1,2},{2,3},{3,4},{4,5},{5,6},{6,7},{7,8},{8,9},{9,10},{10,1... | collective-permute-start | bytes 368 | tf_op jit(solution)/shard_map/ppermute | solution.py:14
  6.0 13.5 %collective-permute-start = (bf16[30,2048]{1,0:T(8,128)(2,1)S(1)}, bf16[30,2048]{1,0:T(8,128)(2,1)S(1)}, u32[]{:S(2)}, u32[]{:S(2)}) collective-permute-start(bf16[30,2048]{1,0:T(8,128)(2,1)S(1)} %slice.388), channel_id=1, source_target_pairs={{0,1},{1,2},{2,3},{3,4},{4,5},{5,6},{6,7},{7,8},{8,9},{9,10},{10,1... | collective-permute-start | bytes 368648 | tf_op jit(solution)/shard_map/ppermute | solution.py:14
  19.5 6.4 %slice-start = ((s8[8388608]{0:T(1024)(128)(4,1)}), s8[4194304]{0:T(1024)(128)(4,1)S(1)}, s32[]{:S(2)}) async-start(s8[8388608]{0:T(1024)(128)(4,1)} %bitcast.170), calls=%async_computation.2 | async-start | bytes 8388608
  19.7 6.2 %slice-start.1 = ((s8[8388608]{0:T(1024)(128)(4,1)}), s8[4194304]{0:T(1024)(128)(4,1)S(1)}, s32[]{:S(2)}) async-start(s8[8388608]{0:T(1024)(128)(4,1)} %bitcast.170), calls=%async_computation.3 | async-start | bytes 8388608
  19.7 6.2 %copy-start.3 = (bf16[128,2048]{1,0:T(8,128)(2,1)S(1)}, bf16[128,2048]{1,0:T(8,128)(2,1)}, u32[]{:S(2)}) copy-start(bf16[128,2048]{1,0:T(8,128)(2,1)} %param.20) | copy-start | bytes 1572868
  19.7 6.2 %copy-start.4 = (f32[2048]{0:T(1024)S(1)}, f32[2048]{0:T(1024)}, u32[]{:S(2)}) copy-start(f32[2048]{0:T(1024)} %param.19) | copy-start | bytes 24580
  19.8 6.2 %copy-start.5 = (f32[2048]{0:T(1024)S(1)}, f32[2048]{0:T(1024)}, u32[]{:S(2)}) copy-start(f32[2048]{0:T(1024)} %param.18) | copy-start | bytes 24580
  26.0 1.8 copy-start.1
  131.6 2.0 copy-start
  175.1 5.4 %copy-start.2 = (f32[128,4]{0,1:T(4,128)S(1)}, f32[128,4]{0,1:T(4,128)}, u32[]{:S(2)}) copy-start(f32[128,4]{0,1:T(4,128)} %param.24) | copy-start | bytes 6148
  175.1 97.8 %all-to-all-start.1 = ((bf16[16,1,64,2048]{3,2,1,0:T(8,128)(2,1)}), bf16[16,1,64,2048]{3,2,1,0:T(8,128)(2,1)}, u32[]{:S(2)}, u32[]{:S(2)}) async-start(bf16[16,1,64,2048]{3,2,1,0:T(8,128)(2,1)} %convert_bitcast_fusion), calls=%async_computation.1 | async-start | bytes 8388608 | tf_op jit(solution)/shard_map/all_to_all | solution.py:107
where the time goes:
time: 290 us; the launch traced here: 289 us
  blocking collectives  97.6 us (34%)
  waiting for transfers between devices  92.3 us (32%)
  matrix products  43.4 us (15%)
  local copies, waits for them, and re-layouts  26.4 us (9%)
  other arithmetic  18.5 us (6%)
  starting transfers between devices  11 us (4%)
    all_to_all x1, blocking collectives, shards(): lax.all_to_all(packed, 'sp', split_axis=0, concat_axis=0, tiled=True)  97.6 us
    all_to_all x1, waiting for transfers between devices, shards(): lax.all_to_all(results, 'sp', split_axis=0, concat_axis=0, tiled=True)  92.3 us
    dot_general x1, matrix products, shards(): jnp.einsum('slmf,lfd->slmd', lax.all_gather(hidden, 'tp', axis=3, tiled=T...  28.4 us
    dot_general x1, matrix products, shards(): jnp.einsum('slmd,ldf->slmf', arrived, glu_weight, preferred_element_type=...  13.2 us
    gather x1, local copies, waits for them, and re-layouts, shards(): flat_back[slot_index].reshape(tok_count, top_count, local_width)  7.13 us
    reduce_sum x1, other arithmetic, shards(): jnp.sum(conv_sum, axis=1)  6.11 us
    gather x1, local copies, waits for them, and re-layouts, shards(): normed_pad[slot_token]  6.02 us
  transfers between devices with their start and end apart: 3, of which 1 were waited for; matrix products, arithmetic and copies ran while one was open for 5% of the time, Pallas kernels for 0%

commit v1 on v0

--- a/solution.py
+++ b/solution.py
@@ -1,6 +1,9 @@
+import functools
 import jax
 import jax.numpy as jnp
 from jax import lax
+from jax.experimental import pallas as pl
+from jax.experimental.pallas import tpu as pltpu
 from jax.sharding import PartitionSpec as P
 
 EPSILON = 1e-05
@@ -20,7 +23,315 @@
     return gate_clip * jax.nn.sigmoid(SIGMOID_SCALE * gate_clip) * (linear + 1.0)
 
 
+def at_place(place, chips, inner):
+    if inner == 1:
+        return place
+    depth = chips // 2
+    column = place // depth
+    return (place * (1 - column) + (chips - 1 - place) * column) * 2 + column
+
+
+def place_of(chip, chips, inner):
+    if inner == 1:
+        return chip
+    column = chip % 2
+    depth = chip // 2
+    return depth * (1 - column) + (chips - 1 - depth) * column
+
+
+def remote(source, target, send_sem, recv_sem, device):
+    return pltpu.make_async_remote_copy(
+        src_ref=source,
+        dst_ref=target,
+        send_sem=send_sem,
+        recv_sem=recv_sem,
+        device_id={"sp": device},
+        device_id_type=pl.DeviceIdType.MESH,
+    )
+
+
+def ring(sp_count, inner):
+    chips = sp_count // 2
+    me = lax.axis_index("sp")
+    core = me % 2
+    place = place_of(me // 2, chips, inner)
+
+    def device_at(by, which=0):
+        other = (core + which) % 2
+        return at_place((place + by + chips) % chips, chips, inner) * 2 + other
+
+    return chips, me, core, device_at
+
+
+def gather_kernel(
+    sp_count, inner, capacity, rows_ref, meta_ref, arrived_ref, rank_ref, weight_ref,
+    gathered, all_meta, near_send, cw_send, ccw_send, row_recv, meta_send, meta_recv,
+):
+    chips, me, core, device_at = ring(sp_count, inner)
+    partner = device_at(0, 1)
+    tok_count = rows_ref.shape[0]
+    half_rows = tok_count // 2
+    far = chips // 2
+
+    barrier = pltpu.get_barrier_semaphore()
+    for by in range(1, sp_count):
+        pl.semaphore_signal(
+            barrier, inc=1, device_id={"sp": (me + by) % sp_count},
+            device_id_type=pl.DeviceIdType.MESH,
+        )
+    pl.semaphore_wait(barrier, sp_count - 1)
+
+    sent = []
+
+    def start(source, owner, half, send_sem, device):
+        copy = remote(
+            source, gathered.at[owner, half], send_sem, row_recv.at[owner, half], device
+        )
+        copy.start()
+        sent.append(copy)
+
+    def landed(owner, half):
+        remote(
+            gathered.at[owner, half], gathered.at[owner, half],
+            near_send.at[0, 0], row_recv.at[owner, half], partner,
+        ).wait_recv()
+
+    def own(half):
+        return rows_ref.at[pl.ds(half * half_rows, half_rows)]
+
+    for half in range(2):
+        start(own(half), me, half, cw_send.at[0, half], device_at(1))
+        start(own(half), me, half, ccw_send.at[0, half], device_at(-1))
+    for by in range(1, sp_count):
+        copy = remote(
+            meta_ref, all_meta.at[me], meta_send.at[by], meta_recv.at[me],
+            (me + by) % sp_count,
+        )
+        copy.start()
+        sent.append(copy)
+    for half in range(2):
+        start(own(half), me, half, near_send.at[me, half], partner)
+    all_meta[me] = meta_ref[...]
+    for by in range(1, sp_count):
+        owner = (me + by) % sp_count
+        remote(
+            all_meta.at[owner], all_meta.at[owner], meta_send.at[0], meta_recv.at[owner], partner
+        ).wait_recv()
+
+    mine = me.astype(jnp.float32)
+    top_count = 4 if meta_ref.shape[0] == 8 else meta_ref.shape[0] // 2
+    named = jnp.zeros((sp_count, tok_count), jnp.float32)
+    weight = jnp.zeros((sp_count, tok_count), jnp.float32)
+    for k in range(top_count):
+        hit = (all_meta[:, k, :] == mine).astype(jnp.float32)
+        named = named + hit
+        weight = weight + hit * all_meta[:, top_count + k, :]
+    upper = (
+        lax.broadcasted_iota(jnp.int32, (tok_count, tok_count), 0)
+        <= lax.broadcasted_iota(jnp.int32, (tok_count, tok_count), 1)
+    ).astype(jnp.bfloat16)
+    rank_ref[...] = named * jnp.dot(
+        named.astype(jnp.bfloat16), upper, preferred_element_type=jnp.float32
+    )
+    weight_ref[...] = weight
+    slots = lax.broadcasted_iota(jnp.int32, (capacity, tok_count), 0).astype(jnp.float32) + 1.0
+
+    def dispatch(owner, lower, upper_rows):
+        chosen = (rank_ref[pl.ds(owner, 1), :] == slots).astype(jnp.bfloat16)
+        total = jnp.dot(
+            chosen[:, :half_rows], lower, preferred_element_type=jnp.float32
+        ) + jnp.dot(chosen[:, half_rows:], upper_rows, preferred_element_type=jnp.float32)
+        arrived_ref[owner] = total.astype(jnp.bfloat16)
+
+    def dispatch_gathered(owner):
+        dispatch(owner, gathered[owner, 0], gathered[owner, 1])
+
+    def dispatch_partner(by):
+        owner = device_at(by, 1)
+        for half in range(2):
+            landed(owner, half)
+        dispatch_gathered(owner)
+
+    dispatch(me, rows_ref[:half_rows], rows_ref[half_rows:])
+    dispatch_partner(0)
+    for step in range(1, far + 1):
+        for half in range(2):
+            for way, sems in ((1, cw_send), (-1, ccw_send)):
+                if step == far and half != (0 if way == 1 else 1):
+                    continue
+                owner = device_at(-way * step)
+                landed(owner, half)
+                block = gathered.at[owner, half]
+                if step + 1 < far or (step + 1 == far and half == (0 if way == 1 else 1)):
+                    start(block, owner, half, sems.at[step, half], device_at(way))
+                start(block, owner, half, near_send.at[owner, half], partner)
+        dispatch_gathered(device_at(step))
+        if step < far:
+            dispatch_gathered(device_at(-step))
+        if step > 1:
+            dispatch_partner(step - 1)
+            dispatch_partner(1 - step)
+    dispatch_partner(far)
+    for copy in sent:
+        copy.wait_send()
+
+
+def gather_rows(rows, meta, sp_count, inner, capacity):
+    tok_count, width = rows.shape
+    far = sp_count // 4
+    vmem = pl.BlockSpec(memory_space=pltpu.VMEM)
+    sems = pltpu.SemaphoreType.DMA
+    return pl.pallas_call(
+        functools.partial(gather_kernel, sp_count, inner, capacity),
+        out_shape=(
+            jax.ShapeDtypeStruct((sp_count, capacity, width), jnp.bfloat16),
+            jax.ShapeDtypeStruct((sp_count, tok_count), jnp.float32),
+            jax.ShapeDtypeStruct((sp_count, tok_count), jnp.float32),
+        ),
+        in_specs=[vmem, vmem],
+        out_specs=(vmem, vmem, vmem),
+        scratch_shapes=[
+            pltpu.VMEM((sp_count, 2, tok_count // 2, width), jnp.bfloat16),
+            pltpu.VMEM((sp_count,) + meta.shape, jnp.float32),
+            sems((sp_count, 2)),
+            sems((far, 2)),
+            sems((far, 2)),
+            sems((sp_count, 2)),
+            sems((sp_count,)),
+            sems((sp_count,)),
+        ],
+        compiler_params=pltpu.CompilerParams(
+            collective_id=1, has_side_effects=True, vmem_limit_bytes=48 * 1024 * 1024
+        ),
+    )(rows, meta)
+
+
+def scatter_kernel(
+    sp_count, inner, results_ref, rank_ref, weight_ref, updated_ref, out_ref,
+    near_out, near_in, ring_out, ring_in, near_send, near_recv, ring_send, ring_recv,
+):
+    chips, me, core, device_at = ring(sp_count, inner)
+    partner = device_at(0, 1)
+    capacity = results_ref.shape[1]
+    tok_count, width = updated_ref.shape
+    part = width // 2
+    far = chips // 2
+
+    barrier = pltpu.get_barrier_semaphore()
+    for device in (partner, device_at(1), device_at(-1)):
+        pl.semaphore_signal(
+            barrier, inc=1, device_id={"sp": device}, device_id_type=pl.DeviceIdType.MESH
+        )
+    pl.semaphore_wait(barrier, 3)
+
+    slots = lax.broadcasted_iota(jnp.int32, (tok_count, capacity), 1).astype(jnp.float32) + 1.0
+
+    def combined(owner, half):
+        chosen = (rank_ref[owner] == slots).astype(jnp.bfloat16)
+        return weight_ref[owner] * jnp.dot(
+            chosen,
+            results_ref[owner, :, half * part : (half + 1) * part],
+            preferred_element_type=jnp.float32,
+        )
+
+    def near_copy(slot, half):
+        return remote(
+            near_out.at[slot, half], near_in.at[slot, half],
+            near_send.at[slot, half], near_recv.at[slot, half], partner,
+        )
+
+    def ring_copy(way, number):
+        return remote(
+            ring_out.at[way, number], ring_in.at[way, number],
+            ring_send.at[way, number], ring_recv.at[way, number],
+            device_at(1 if way == 0 else -1),
+        )
+
+    def give(by, half):
+        slot = by % chips
+        near_out[slot, half] = combined(device_at(by, 1), half).astype(jnp.bfloat16)
+        near_copy(slot, half).start()
+
+    def own_sum(by, half):
+        slot = by % chips
+        mine = combined(device_at(by), half)
+        near_copy(slot, half).wait_recv()
+        return mine + near_in[slot, half].astype(jnp.float32)
+
+    plan = [(far, 0), (far - 1, 1)]
+    while plan[-2][0] > 1 or plan[-1][0] > 1:
+        distance, half = plan[-2]
+        plan.append((distance - 1, half))
+        if len(plan) > 4 * far:
+            break
+    plan = [(distance, half) for distance, half in plan if distance >= 1]
+
+    for distance, half in plan:
+        give(distance, half)
+        give(-distance, 1 - half)
+    give(0, 0)
+    give(0, 1)
+    for number, (distance, half) in enumerate(plan):
+        for way in range(2):
+            by = distance if way == 0 else -distance
+            column_half = half if way == 0 else 1 - half
+            total = own_sum(by, column_half)
+            if number >= 2:
+                ring_copy(way, number - 2).wait_recv()
+                total = total + ring_in[way, number - 2].astype(jnp.float32)
+            ring_out[way, number] = total.astype(jnp.bfloat16)
+            ring_copy(way, number).start()
+    finals = len(plan)
+    totals = [own_sum(0, 0), own_sum(0, 1)]
+    for number in (finals - 2, finals - 1):
+        half = plan[number][1]
+        for way in range(2):
+            ring_copy(way, number).wait_recv()
+            column_half = half if way == 0 else 1 - half
+            totals[column_half] = totals[column_half] + ring_in[way, number].astype(jnp.float32)
+    for half in range(2):
+        columns = slice(half * part, (half + 1) * part)
+        out_ref[:, columns] = (
+            updated_ref[:, columns].astype(jnp.float32) + totals[half]
+        ).astype(jnp.bfloat16)
+    for slot in range(chips):
+        for half in range(2):
+            near_copy(slot, half).wait_send()
+    for number in range(finals):
+        for way in range(2):
+            ring_copy(way, number).wait_send()
+
+
+def scatter_sums(results, rank, weight, updated, sp_count, inner):
+    tok_count, width = updated.shape
+    chips = sp_count // 2
+    messages = chips - 1
+    vmem = pl.BlockSpec(memory_space=pltpu.VMEM)
+    sems = pltpu.SemaphoreType.DMA
+    part = width // 2
+    return pl.pallas_call(
+        functools.partial(scatter_kernel, sp_count, inner),
+        out_shape=jax.ShapeDtypeStruct((tok_count, width), jnp.bfloat16),
+        in_specs=[vmem] * 4,
+        out_specs=vmem,
+        scratch_shapes=[
+            pltpu.VMEM((chips, 2, tok_count, part), jnp.bfloat16),
+            pltpu.VMEM((chips, 2, tok_count, part), jnp.bfloat16),
+            pltpu.VMEM((2, messages, tok_count, part), jnp.bfloat16),
+            pltpu.VMEM((2, messages, tok_count, part), jnp.bfloat16),
+            sems((chips, 2)),
+            sems((chips, 2)),
+            sems((2, messages)),
+            sems((2, messages)),
+        ],
+        compiler_params=pltpu.CompilerParams(
+            collective_id=2, has_side_effects=True, vmem_limit_bytes=48 * 1024 * 1024
+        ),
+    )(results, rank, weight, updated)
+
+
 def shards(
+    inner,
     glu_value,
     glu_gate,
     segments,
@@ -45,12 +356,21 @@
     sp_count = lax.axis_size("sp")
     expert_total = local_experts * sp_count
     capacity = min(tok_count, 2 * tok_count * top_count // expert_total)
+    meta = jnp.concatenate([experts.astype(jnp.float32).T, route_weights.T], axis=0)
     glu_out = (glu_value.astype(jnp.float32) * jax.nn.sigmoid(glu_gate.astype(jnp.float32))).astype(
         jnp.bfloat16
     )
-    prev_rows, prev_segments = passed_along(
-        (glu_out[tok_count - kernel_reach :], segments[tok_count - kernel_reach :]), "sp", 1
-    )
+    tail_segments = segments[tok_count - kernel_reach :].astype(jnp.bfloat16) + 1
+    tail = jnp.concatenate(
+        [
+            glu_out[tok_count - kernel_reach :],
+            jnp.pad(tail_segments, (0, local_width - kernel_reach))[None],
+        ],
+        axis=0,
+    )
+    previous = passed_along(tail, "sp", 1)
+    prev_rows = previous[:kernel_reach]
+    prev_segments = previous[kernel_reach, :kernel_reach].astype(jnp.int32) - 1
     padded = jnp.concatenate([prev_rows, glu_out], axis=0).astype(jnp.float32)
     padded_segments = jnp.concatenate([prev_segments, segments], axis=0)
     conv_sum = jnp.zeros((tok_count, local_width), jnp.float32)
@@ -74,16 +394,6 @@
     ).astype(jnp.float32)
     updated = (residual.astype(jnp.float32) + conv_out).astype(jnp.bfloat16)
     updated_float = updated.astype(jnp.float32)
-    flat_experts = experts.reshape(-1)
-    one_hot = (flat_experts[:, None] == jnp.arange(expert_total, dtype=jnp.int32)[None, :]).astype(
-        jnp.int32
-    )
-    slot_rank = jnp.sum((jnp.cumsum(one_hot, axis=0) - 1) * one_hot, axis=1)
-    slot_index = flat_experts * capacity + slot_rank
-    token_order = jnp.arange(tok_count * top_count, dtype=jnp.int32) // top_count
-    slot_token = (
-        jnp.full((expert_total * capacity,), tok_count, jnp.int32).at[slot_index].set(token_order)
-    )
     whole_rows = lax.all_gather(updated, "tp", axis=1, tiled=True)
     whole_float = whole_rows.astype(jnp.float32)
     normed = (
@@ -91,9 +401,8 @@
         * lax.rsqrt(jnp.mean(whole_float * whole_float, axis=1, keepdims=True) + EPSILON)
         * rms_gain
     ).astype(jnp.bfloat16)
-    normed_pad = jnp.concatenate([normed, jnp.zeros((1, model_width), jnp.bfloat16)], axis=0)
-    packed = normed_pad[slot_token].reshape(sp_count, local_experts, capacity, model_width)
-    arrived = lax.all_to_all(packed, "sp", split_axis=0, concat_axis=0, tiled=True)
+    arrived, rank, weight = gather_rows(normed, meta, sp_count, inner, capacity)
+    arrived = arrived[:, None]
     gate_pre = jnp.einsum("slmd,ldf->slmf", arrived, glu_weight, preferred_element_type=jnp.float32)
     lin_pre = jnp.einsum("slmd,ldf->slmf", arrived, lin_weight, preferred_element_type=jnp.float32)
     hidden = clamped_unit(gate_pre, lin_pre).astype(jnp.bfloat16)
@@ -103,12 +412,8 @@
         down_weight,
         preferred_element_type=jnp.float32,
     )
-    results = summed.astype(jnp.bfloat16)
-    returned = lax.all_to_all(results, "sp", split_axis=0, concat_axis=0, tiled=True)
-    flat_back = returned.reshape(expert_total * capacity, local_width)
-    picked = flat_back[slot_index].reshape(tok_count, top_count, local_width).astype(jnp.float32)
-    routed_sum = jnp.sum(picked * route_weights[:, :, None], axis=1)
-    return (updated_float + routed_sum).astype(jnp.bfloat16)
+    results = summed[:, 0].astype(jnp.bfloat16)
+    return scatter_sums(results, rank[:, :, None], weight[:, :, None], updated, sp_count, inner)
 
 
 def solution(mesh):
@@ -129,4 +434,7 @@
         P("sp", None, "tp"),
     )
     out_specs = P(("grp", "sp"), "tp")
-    return jax.shard_map(shards, mesh=mesh, in_specs=in_specs, out_specs=out_specs, check_vma=False)
+    coords = [getattr(d, "coords", (0, 0, 0)) for d in mesh.devices[0, :, 0]]
+    inner = len({c[0] for c in coords})
+    body = functools.partial(shards, inner)
+    return jax.shard_map(body, mesh=mesh, in_specs=in_specs, out_specs=out_specs, check_vma=False)

time: 290 us -> 174 us (0.60); the launches traced: 289 us -> 170 us
  Pallas kernels: 0 us -> 102 us
  blocking collectives: 97.6 us -> 0 us
  waiting for transfers between devices: 92.3 us -> 0.01 us
  local copies, waits for them, and re-layouts: 26.4 us -> 7.03 us
  starting transfers between devices: 11 us -> 3.74 us
  other arithmetic: 18.5 us -> 12.3 us
    pallas_call x0 -> x2, Pallas kernels: none -> 102 us  [the longest x1 52.4 us: gather_rows(): pl.pallas_call(functools.partial(gather_kernel, sp_count, inner, capacity...]
    all_to_all x1 -> x0, blocking collectives: 97.6 us -> none  [shards(): lax.all_to_all(packed, 'sp', split_axis=0, concat_axis=0, tiled=True)]
    all_to_all x1 -> x0, waiting for transfers between devices: 92.3 us -> none  [shards(): lax.all_to_all(results, 'sp', split_axis=0, concat_axis=0, tiled=True)]
    gather x2 -> x0, local copies, waits for them, and re-layouts: 13.2 us -> none  [the longest x1 7.13 us: shards(): flat_back[slot_index].reshape(tok_count, top_count, local_width)]
    reduce_sum x2 -> x0, other arithmetic: 5.52 us -> none  [the longest x1 5.42 us: shards(): routed_sum = jnp.sum(picked * route_weights[:, :, None], axis=1)]
    all_to_all x1 -> x0, starting transfers between devices: 5.35 us -> none  [shards(): lax.all_to_all(results, 'sp', split_axis=0, concat_axis=0, tiled=True)]
    convert_element_type x1 -> x0, local copies, waits for them, and re-layouts: 3.03 us -> none  [shards(): flat_back[slot_index].reshape(tok_count, top_count, local_width)]
  transfers between devices with their start and end apart: 3 -> 1, of which waited for: 1 -> 0; matrix products, arithmetic and copies ran while one was open for 5% -> 3% of each run, Pallas kernels for 0% -> 0%
where the time goes in v1:
time: 174 us; the launch traced here: 170 us
  Pallas kernels  102 us (59%)
  matrix products  44.6 us (26%)
  other arithmetic  12.3 us (7%)
  local copies, waits for them, and re-layouts  7.03 us (4%)
  starting transfers between devices  3.74 us (2%)
    pallas_call x1, Pallas kernels, gather_rows(): pl.pallas_call(functools.partial(gather_kernel, sp_count, inner, capacity...  52.4 us
    pallas_call x1, Pallas kernels, scatter_sums(): pl.pallas_call(functools.partial(scatter_kernel, sp_count, inner), out_sh...  49.9 us
    dot_general x1, matrix products, shards(): jnp.einsum('slmf,lfd->slmd', lax.all_gather(hidden, 'tp', axis=3, tiled=T...  28.4 us
    dot_general x1, matrix products, shards(): jnp.einsum('slmd,ldf->slmf', arrived, glu_weight, preferred_element_type=...  14.4 us
    reduce_sum x1, other arithmetic, shards(): jnp.sum(conv_sum, axis=1)  6.1 us
    ppermute x1, starting transfers between devices, passed_along(): return lax.ppermute(array, axis, pairs)  3.74 us
  transfers between devices with their start and end apart: 1, of which 0 were waited for; matrix products, arithmetic and copies ran while one was open for 3% of the time, Pallas kernels for 0%

profile of v1, /device:TPU:11, one launch (start us, length us, event | category | flops | bytes accessed | tf_op | source)
XLA Modules:
  0.0 170.3 jit_solution(9202161684965312419)
XLA Ops:
  0.0 1.5 multiply_convert_fusion.1
  1.5 0.7 convert.3
  2.2 0.1 slice_add_fusion
  2.3 3.7 %collective-permute-start = (bf16[31,2048]{1,0:T(8,128)(2,1)S(1)}, bf16[31,2048]{1,0:T(8,128)(2,1)S(1)}, u32[]{:S(2)}, u32[]{:S(2)}) collective-permute-start(bf16[31,2048]{1,0:T(8,128)(2,1)S(1)} %pad_maximum_fusion), channel_id=1, source_target_pairs={{0,1},{1,2},{2,3},{3,4},{4,5},{5,6},{6,7},{7,8},{8,9},{9,10},{10,1... | collective-permute-start | bytes 380936 | tf_op jit(solution)/shard_map/ppermute | solution.py:17
  6.1 2.0 %fusion.110 = (f32[1,2048]{1,0:T(1,128)S(1)}, f32[1,2048]{1,0:T(1,128)S(1)}, f32[1,2048]{1,0:T(1,128)S(1)}, f32[1,2048]{1,0:T(1,128)S(1)}, f32[1,2048]{1,0:T(1,1...) fusion(f32[31,2048]{1,0:T(8,128)} %param.17), kind=kLoop, calls=%fused_computation.177 | loop fusion | bytes 311296 | tf_op jit(solution)/shard_map/slice | solution.py:381
  8.0 1.5 fusion.111
  9.5 0.7 convert_bitcast_fusion
  10.2 0.7 pad_maximum_fusion.1.meta_ref
  10.9 0.7 pad_add_fusion
  11.6 0.7 compare_convert_fusion.29
  12.4 0.7 compare_convert_fusion.28
  13.1 0.2 maximum_convert_fusion
  13.3 0.0 slice-start.1
  13.4 6.1 %fusion.108 = (f32[128]{0:T(128)S(1)}, f32[128]{0:T(128)S(1)}, f32[128,2048]{1,0:T(8,128)S(1)}) fusion(f32[128]{0:T(128)S(1)} %get-tuple-element.73, f32[158,2048]{1,0:T(8,128)S(1)} %maximum_convert_fusion, f32[2048]{0:T(1024)S(1)} %bitcast.140, f32[128]{0:T(128)S(1)} %get-tuple-element.74, f32[2048]{0:T(1024)S(1)} %bitcast.141, ...), kind=kLoop, calls=%fused_computation.176 | loop fusion | flops 24641280 | bytes 33824768 | tf_op jit(solution)/shard_map/reduce_sum | solution.py:383
  19.6 1.8 %fusion.33 = (f32[128]{0:T(128)S(1)}, bf16[128,2048]{1,0:T(8,128)(2,1)S(1)}) fusion(bf16[2048,2048]{1,0:T(8,128)(2,1)S(1)} %bitcast.144, f32[128,2048]{1,0:T(8,128)S(1)} %get-tuple-element.13, f32[2048]{0:T(1024)S(1)} %copy-done.3, f32[2048]{0:T(1024)S(1)} %copy-done.4, f32[128]{0:T(128)S(1)} %get-tuple-element.76, f32[128]{0:T(128)S(1)} %get-tuple-element.75, ...), kind=kOutput, calls=%fused_computation.27 | convolution fusion | flops 1078198144 | bytes 10503680 | tf_op jit(solution)/shard_map/dot_general | solution.py:391
  21.4 0.2 fusion.35.rows_ref
  21.6 52.4 %shard_map.136 = (bf16[16,64,2048]{2,1,0:T(8,128)(2,1)S(1)}, f32[16,128]{1,0:T(8,128)S(1)}, f32[16,128]{1,0:T(8,128)S(1)}) custom-call(bf16[128,2048]{1,0:T(8,128)(2,1)S(1)} %fusion.35.rows_ref, f32[8,128]{1,0:T(8,128)S(1)} %pad_maximum_fusion.1.meta_ref), custom_call_target="tpu_custom_call" | custom-call | tf_op jit(solution)/shard_map/pallas_call | solution.py:184
  74.0 2.0 %copy-done = bf16[16,64,2048]{2,1,0:T(8,128)(2,1)} copy-done((bf16[16,64,2048]{2,1,0:T(8,128)(2,1)}, bf16[16,64,2048]{2,1,0:T(8,128)(2,1)S(1)}, u32[]{:S(2)}) %copy-start) | copy-done | bytes 4194328
  76.0 0.4 copy.15.rank_ref
  76.4 0.4 copy.16.weight_ref
  76.7 14.4 %fusion.9 = f32[16,64,2048]{2,1,0:T(8,128)} fusion(bf16[16,64,2048]{2,1,0:T(8,128)(2,1)} %copy-done, bf16[1,2048,2048]{2,1,0:T(8,128)(2,1)} %param.25), kind=kOutput, calls=%fused_computation.12 | convolution fusion | flops 8589934592 | bytes 20971520 | tf_op jit(solution)/shard_map/slmd,ldf->slmf/dot_general | solution.py:406
  91.2 28.4 %fusion.23.results_ref = bf16[16,64,2048]{2,1,0:T(8,128)(2,1)} fusion(bf16[1,2048,2048]{2,1,0:T(8,128)(2,1)} %param.27, bf16[16,64,2048]{2,1,0:T(8,128)(2,1)} %copy-done, bf16[1,2048,2048]{2,1,0:T(8,128)(2,1)} %param.26, f32[16,64,2048]{2,1,0:T(8,128)} %fusion.9), kind=kOutput, calls=%fused_computation.20 | convolution fusion | flops 17202937856 | bytes 33554432 | tf_op jit(solution)/shard_map/slmf,lfd->slmd/dot_general | solution.py:409
  119.6 49.9 %shard_map.137 = bf16[128,2048]{1,0:T(8,128)(2,1)S(1)} custom-call(bf16[16,64,2048]{2,1,0:T(8,128)(2,1)} %fusion.23.results_ref, f32[16,128,1]{2,1,0:T(8,128)S(1)} %copy.15.rank_ref, f32[16,128,1]{2,1,0:T(8,128)S(1)} %copy.16.weight_ref, bf16[128,2048]{1,0:T(8,128)(2,1)S(1)} %get-tuple-element.78.updated_ref), custom_call_target="tpu_custom_call" | custom-call | tf_op jit(solution)/shard_map/pallas_call | solution.py:312
  169.5 0.8 copy.18
  (21 shorter events, 0.1 us)
Async XLA Ops:
  2.3 8.6 %collective-permute-start = (bf16[31,2048]{1,0:T(8,128)(2,1)S(1)}, bf16[31,2048]{1,0:T(8,128)(2,1)S(1)}, u32[]{:S(2)}, u32[]{:S(2)}) collective-permute-start(bf16[31,2048]{1,0:T(8,128)(2,1)S(1)} %pad_maximum_fusion), channel_id=1, source_target_pairs={{0,1},{1,2},{2,3},{3,4},{4,5},{5,6},{6,7},{7,8},{8,9},{9,10},{10,1... | collective-permute-start | bytes 380936 | tf_op jit(solution)/shard_map/ppermute | solution.py:17
  13.1 6.4 %slice-start = ((s8[8388608]{0:T(1024)(128)(4,1)}), s8[4194304]{0:T(1024)(128)(4,1)S(1)}, s32[]{:S(2)}) async-start(s8[8388608]{0:T(1024)(128)(4,1)} %bitcast.143), calls=%async_computation | async-start | bytes 8388608
  13.3 6.2 %slice-start.1 = ((s8[8388608]{0:T(1024)(128)(4,1)}), s8[4194304]{0:T(1024)(128)(4,1)S(1)}, s32[]{:S(2)}) async-start(s8[8388608]{0:T(1024)(128)(4,1)} %bitcast.143), calls=%async_computation.1 | async-start | bytes 8388608
  13.3 6.2 %copy-start.2 = (bf16[128,2048]{1,0:T(8,128)(2,1)S(1)}, bf16[128,2048]{1,0:T(8,128)(2,1)}, u32[]{:S(2)}) copy-start(bf16[128,2048]{1,0:T(8,128)(2,1)} %param.20) | copy-start | bytes 1572868
  13.3 6.2 %copy-start.3 = (f32[2048]{0:T(1024)S(1)}, f32[2048]{0:T(1024)}, u32[]{:S(2)}) copy-start(f32[2048]{0:T(1024)} %param.19) | copy-start | bytes 24580
  13.4 6.2 %copy-start.4 = (f32[2048]{0:T(1024)S(1)}, f32[2048]{0:T(1024)}, u32[]{:S(2)}) copy-start(f32[2048]{0:T(1024)} %param.18) | copy-start | bytes 24580
  19.6 1.8 %copy-start.1 = (f32[2048]{0:T(1024)S(1)}, f32[2048]{0:T(1024)}, u32[]{:S(2)}) copy-start(f32[2048]{0:T(1024)} %param.22) | copy-start | bytes 24580
  74.0 2.0 %copy-start = (bf16[16,64,2048]{2,1,0:T(8,128)(2,1)}, bf16[16,64,2048]{2,1,0:T(8,128)(2,1)S(1)}, u32[]{:S(2)}) copy-start(bf16[16,64,2048]{2,1,0:T(8,128)(2,1)S(1)} %get-tuple-element.8) | copy-start | bytes 12582916
